TPU v7x, 32 devices: a whole 2x2x4 slice. The times are simulated.
32 devices in a mesh: ep: 8 (over z, core), tp: 4 (over y, x).
Axes of the slice: x: 2, y: 2, z: 4, core: 2. Of those that a mesh axis runs over, the one named last changes fastest.
Arguments:
- query_rows: bfloat16 [6144, 1024], P('ep', 'tp'), may hold values from -600 to 600
- key_rows: bfloat16 [6144, 1024], P('ep', 'tp'), may hold values from -6 to 6
- value_rows: bfloat16 [6144, 1024], P('ep', 'tp'), may hold values from -6 to 6
- cum_gate: float32 [16, 6144], P('tp'), may hold values from -615 to 0, as said below
- out_weight: bfloat16 [1024, 2048], P(None, 'tp'), may hold values from -0.1875 to 0.1875
- moe_input: bfloat16 [1536, 2048], P('ep'), may hold values from -6 to 6
- moe_gain: float32 [2048], replicated, may hold values from 0.1 to 1.9
- routes: int32 [1536, 3], P('ep'), may hold values from 0 to 31, all different within a row; in each aligned block of 192 rows (0 to 191, 192 to 383, ...) at most 36 rows name the same one
- route_weight: float32 [1536, 3], P('ep'), may hold values from 0.2 to 1.5
- expert_gate: bfloat16 [32, 2048, 512], P('ep', None, 'tp'), may hold values from -0.125 to 0.125
- expert_up: bfloat16 [32, 2048, 512], P('ep', None, 'tp'), may hold values from -0.125 to 0.125
- expert_down: bfloat16 [32, 512, 2048], P('ep', None, 'tp'), may hold values from -0.25 to 0.25
- shared_gate: bfloat16 [2048, 512], P(None, 'tp'), may hold values from -0.125 to 0.125
- shared_up: bfloat16 [2048, 512], P(None, 'tp'), may hold values from -0.125 to 0.125
- shared_down: bfloat16 [512, 2048], P(None, 'tp'), may hold values from -0.25 to 0.25
Outputs:
- mixer_out: bfloat16 [6144, 2048], P('ep', 'tp')
- moe_out: bfloat16 [1536, 2048], P('ep', 'tp')
Inputs may be any that keep to these rules, and one draw needn't show every extreme that they name: Non-increasing along positions: cum_gate[h, t] is the sum of the log forget gates of head h over positions 0 to t. `routes`: the 3 experts of a token differ. In each aligned block of 192 tokens no expert is named by more than 36 tokens, a bound that some block reaches.
All inputs are finite; a program needn't handle non-finite values.
Results may differ from a plain program's by a relative error of at most 0.0068.
Values may be sent and summed in bfloat16 or wider, within the bound.
A program may use at most 64 MiB of HBM per device.

v0:
```python
import jax
import jax.numpy as jnp
from jax import lax
from jax.sharding import PartitionSpec as P

HEAD = 64
neg_fill = -1e30
norm_eps = 1e-06


def local(
    query_rows,
    key_rows,
    value_rows,
    cum_gate,
    out_weight,
    moe_input,
    moe_gain,
    routes,
    route_weight,
    expert_gate,
    expert_up,
    expert_down,
    shared_gate,
    shared_up,
    shared_down,
):
    row_count = query_rows.shape[0]
    width = query_rows.shape[1]
    local_heads = width // HEAD
    scale = HEAD ** (-0.5)
    first_row = lax.axis_index("ep") * row_count
    last_row = first_row + row_count - 1
    query_heads = query_rows.reshape(row_count, local_heads, HEAD)
    query_gate = lax.dynamic_slice_in_dim(cum_gate, first_row, row_count, 1)
    query_pos = first_row + jnp.arange(row_count, dtype=jnp.int32)
    key_value = jnp.concatenate([key_rows, value_rows], axis=1)
    initial = (
        jnp.full((local_heads, row_count), neg_fill, jnp.float32),
        jnp.zeros((local_heads, row_count), jnp.float32),
        jnp.zeros((local_heads, row_count, HEAD), jnp.float32),
    )
    shard_rows = lax.all_gather(key_value, "ep", axis=0, tiled=True)
    piece_len = shard_rows.shape[0]
    key_span = 512

    def one_span(state_in, span_index):
        span_start = span_index * key_span

        def update(state_old):
            running_max, denominator, weighted = state_old
            block = lax.dynamic_slice_in_dim(shard_rows, span_index * key_span, key_span, 0)
            keys_block = block[:, :width].reshape(key_span, local_heads, HEAD)
            values_block = block[:, width:].reshape(key_span, local_heads, HEAD)
            key_gate = lax.dynamic_slice_in_dim(cum_gate, span_start, key_span, 1)
            scores = (
                jnp.einsum(
                    "qhd,khd->hqk", query_heads, keys_block, preferred_element_type=jnp.float32
                )
                * scale
            )
            scores = scores + query_gate[:, :, None] - key_gate[:, None, :]
            causal = (span_start + jnp.arange(key_span, dtype=jnp.int32))[None, :] <= query_pos[
                :, None
            ]
            scores = jnp.where(causal[None], scores, neg_fill)
            new_max = jnp.maximum(running_max, jnp.max(scores, axis=2))
            expon = jnp.where(causal[None], jnp.exp(scores - new_max[:, :, None]), 0.0)
            rescale = jnp.exp(running_max - new_max)
            denominator = denominator * rescale + jnp.sum(expon, axis=2)
            weighted = weighted * rescale[:, :, None] + jnp.einsum(
                "hqk,khd->hqd",
                expon.astype(jnp.bfloat16),
                values_block,
                preferred_element_type=jnp.float32,
            )
            return (new_max, denominator, weighted)

        state_next = lax.cond(span_start <= last_row, update, lambda unchanged: unchanged, state_in)
        return (state_next, None)

    state_out, _ = lax.scan(one_span, initial, jnp.arange(piece_len // key_span, dtype=jnp.int32))
    running_max, denominator, weighted = state_out
    heads_out = (weighted / denominator[:, :, None]).transpose(1, 0, 2).reshape(row_count, width)
    heads_out = heads_out.astype(jnp.bfloat16)
    token_count = moe_input.shape[0]
    top_count = routes.shape[1]
    local_experts = expert_gate.shape[0]
    ep_count = lax.axis_size("ep")
    expert_count = local_experts * ep_count
    capacity = 2 * token_count * top_count // expert_count
    column_count = expert_down.shape[2]
    first_column = lax.axis_index("tp") * column_count
    moe_rows = moe_input.astype(jnp.float32)
    normed = (
        moe_rows
        * lax.rsqrt(jnp.mean(moe_rows * moe_rows, axis=1, keepdims=True) + norm_eps)
        * moe_gain
    ).astype(jnp.bfloat16)
    flat_routes = routes.reshape(-1)
    one_hot = (flat_routes[:, None] == jnp.arange(expert_count, dtype=jnp.int32)[None, :]).astype(
        jnp.int32
    )
    ranks = jnp.sum(jnp.cumsum(one_hot, axis=0) * one_hot, axis=1) - 1
    slot_index = flat_routes * capacity + ranks
    pair_token = jnp.arange(token_count * top_count, dtype=jnp.int32) // top_count
    slot_token = (
        jnp.full((expert_count * capacity,), token_count, jnp.int32).at[slot_index].set(pair_token)
    )
    padded = jnp.concatenate([normed, jnp.zeros((1, normed.shape[1]), jnp.bfloat16)], axis=0)
    outgoing = lax.dynamic_slice_in_dim(padded, first_column, column_count, 1)[slot_token]
    outgoing = outgoing.reshape(ep_count, local_experts, capacity, outgoing.shape[1])
    arrived = lax.all_to_all(outgoing, "ep", split_axis=0, concat_axis=0, tiled=True)
    arrived = lax.all_gather(arrived, "tp", axis=3, tiled=True)
    gate_val = jnp.einsum(
        "aecd,edf->aecf", arrived, expert_gate, preferred_element_type=jnp.float32
    )
    up_val = jnp.einsum("aecd,edf->aecf", arrived, expert_up, preferred_element_type=jnp.float32)
    hidden = (jax.nn.silu(gate_val) * up_val).astype(jnp.bfloat16)
    hidden = lax.all_gather(hidden, "tp", axis=3, tiled=True)
    result = jnp.einsum(
        "aecf,efd->aecd", hidden, expert_down, preferred_element_type=jnp.float32
    ).astype(jnp.bfloat16)
    returned = lax.all_to_all(result, "ep", split_axis=0, concat_axis=0, tiled=True)
    picked = returned.reshape(expert_count * capacity, column_count)[slot_index]
    picked = picked.astype(jnp.float32).reshape(token_count, top_count, column_count)
    routed = jnp.sum(picked * route_weight[:, :, None], axis=1)
    shared_hidden = (
        jax.nn.silu(jnp.dot(normed, shared_gate, preferred_element_type=jnp.float32))
        * jnp.dot(normed, shared_up, preferred_element_type=jnp.float32)
    ).astype(jnp.bfloat16)
    heads_all, shared_all = (
        lax.all_gather(heads_out, "tp", axis=1, tiled=True),
        lax.all_gather(shared_hidden, "tp", axis=1, tiled=True),
    )
    mixer_sum = jnp.dot(heads_all, out_weight, preferred_element_type=jnp.float32)
    moe_total = routed + jnp.dot(shared_all, shared_down, preferred_element_type=jnp.float32)
    return (mixer_sum.astype(jnp.bfloat16), moe_total.astype(jnp.bfloat16))


def solution(mesh):
    placed = (
        P("ep", "tp"),
        P("ep", "tp"),
        P("ep", "tp"),
        P("tp", None),
        P(None, "tp"),
        P("ep", None),
        P(),
        P("ep", None),
        P("ep", None),
        P("ep", None, "tp"),
        P("ep", None, "tp"),
        P("ep", None, "tp"),
        P(None, "tp"),
        P(None, "tp"),
        P(None, "tp"),
    )
    return jax.shard_map(
        local, mesh=mesh, in_specs=placed, out_specs=(P("ep", "tp"), P("ep", "tp")), check_vma=False
    )
```

profile of v0, /device:TPU:0, one launch (start us, length us, event | category | flops | bytes accessed | tf_op | source)
XLA Modules:
  0.0 447.6 jit_solution(2679872729784148897)
XLA Ops:
  7.2 0.8 broadcast_multiply_fusion
  8.9 1.4 fusion.23
  10.8 1.5 reduce-window.6
  12.8 4.1 scatter_custom_fusion
  16.9 1.4 fusion.25
  18.3 4.7 %gather_fusion = bf16[1152,512]{1,0:T(8,128)(2,1)} fusion(bf16[193,512]{1,0:T(8,128)(2,1)S(1)} %pad_dynamic-slice_fusion, s32[2048]{0:T(1024)S(1)} %pad_clamp_fusion), kind=kCustom, calls=%fused_computation | custom fusion | bytes 2363904 | tf_op jit(solution)/shard_map/gather | solution.py:111
  23.0 2.9 reshape.119
  25.9 1.9 copy.41
  27.9 35.5 %all_to_all.10 = bf16[8,4,36,512]{3,1,2,0:T(4,128)(2,1)S(1)} all-to-all(bf16[8,4,36,512]{3,1,2,0:T(4,128)(2,1)S(1)} %copy.41), channel_id=1, replica_groups=mesh['ep'=8,'tp'=4] {'ep'}, dimensions={0} | all-to-all | bytes 2359296 | tf_op jit(solution)/shard_map/all_to_all | solution.py:113
  63.4 1.4 copy.42
  64.8 60.2 %all-gather.9.cloned.1.call-done = bf16[8,4,36,2048]{3,2,0,1:T(8,128)(2,1)} async-done(((bf16[8,4,36,512]{3,2,0,1:T(8,128)(2,1)}), bf16[8,4,36,2048]{3,2,0,1:T(8,128)(2,1)}) %all-gather.9.cloned.1.call-update) | async-done | bytes 4718608 | tf_op jit(solution)/shard_map/all_gather | solution.py:114
  125.0 4.8 %fusion.29 = f32[8,4,36,128]{3,2,0,1:T(8,128)S(1)} fusion(bf16[8,4,36,2048]{3,2,0,1:T(8,128)(2,1)} %all-gather.9.cloned.1.call-done, bf16[4,2048,128]{2,1,0:T(8,128)(2,1)} %param.28), kind=kOutput, calls=%fused_computation.37 | convolution fusion | flops 603979776 | bytes 7405568 | tf_op jit(solution)/shard_map/aecd,edf->aecf/dot_general | solution.py:115
  130.3 2.3 fusion.38
  132.7 1.2 copy.35
  133.9 1.9 copy.34
  135.8 1.9 pad_maximum_fusion
  137.7 1.9 copy.36
  140.4 21.0 %all-gather.11.cloned.1.call-done = bf16[8,4,36,512]{3,2,0,1:T(8,128)(2,1)} async-done(((bf16[8,4,36,128]{3,2,0,1:T(8,128)(2,1)}), bf16[8,4,36,512]{3,2,0,1:T(8,128)(2,1)}) %all-gather.11.cloned.1.call-update) | async-done | bytes 1179664 | tf_op jit(solution)/shard_map/all_gather | solution.py:120
  161.3 2.2 fusion.26
  163.5 2.0 copy.43
  165.5 4.6 %all-to-all-start.1 = ((bf16[8,4,36,512]{3,1,2,0:T(4,128)(2,1)}), bf16[8,4,36,512]{3,1,2,0:T(4,128)(2,1)}, u32[]{:S(2)}, u32[]{:S(2)}) async-start(bf16[8,4,36,512]{3,1,2,0:T(4,128)(2,1)} %copy.43), calls=%async_computation.1 | async-start | bytes 2359296 | tf_op jit(solution)/shard_map/all_to_all | solution.py:124
  170.3 81.3 %all-gather.5.cloned.1.call-done = bf16[6144,512]{0,1:T(8,128)(2,1)} async-done(((bf16[768,512]{0,1:T(8,128)(2,1)}), bf16[6144,512]{0,1:T(8,128)(2,1)}) %all-gather.5.cloned.1.call-update) | async-done | bytes 6291472 | tf_op jit(solution)/shard_map/all_gather | solution.py:43
  251.6 0.9 broadcast_in_dim.51
  252.6 39.0 %while.15 = (s32[]{:T(128)}, f32[4,768]{1,0:T(4,128)S(1)}, f32[4,768]{1,0:T(4,128)S(1)}, f32[4,768,64]{1,2,0:T(8,128)}, s32[12]{0:T(128)S(1)}, /*index=5*/s32[]{...) while((s32[]{:T(128)}, f32[4,768]{1,0:T(4,128)S(1)}, ...), condition=%wide.region_5.6_spmd.clone, body=%wide.region_0.5_spmd.clone.sunk | while | flops 433331456 | bytes 30568932 | solution.py:82
  253.9 11.5 %conditional.3 = ((f32[4,768]{1,0:T(4,128)S(1)}, f32[4,768]{1,0:T(4,128)S(1)}, f32[4,768,64]{1,2,0:T(8,128)})) conditional(s32[]{:T(128)} %convert_element_type.85, (f32[4,768]{1,0:T(4,128)S(1)}, f32[4,768]{1,0:T(4,128)S(1)}, f32[4,768,64]{1,2,0:T(8,128)}) %tuple.39, (s32[]{:T(128)}, s32[]{:T(128)}, s32[]{:T(128)}, bf16[6144,512]{0,1:T(8,128)(2,1)}, ...), branch_computations={%region_1.1_spmd, %region_2.4_spmd} | conditional | flops 433331456 | bytes 30565576 | solution.py:79
  255.6 1.1 fusion.50
  256.7 2.9 fusion.4
  259.6 2.3 fusion.3
  262.0 2.5 fusion.8
  264.5 0.9 copy-done.3
  266.7 11.5 %conditional.3 = ((f32[4,768]{1,0:T(4,128)S(1)}, f32[4,768]{1,0:T(4,128)S(1)}, f32[4,768,64]{1,2,0:T(8,128)})) conditional(s32[]{:T(128)} %convert_element_type.85, (f32[4,768]{1,0:T(4,128)S(1)}, f32[4,768]{1,0:T(4,128)S(1)}, f32[4,768,64]{1,2,0:T(8,128)}) %tuple.39, (s32[]{:T(128)}, s32[]{:T(128)}, s32[]{:T(128)}, bf16[6144,512]{0,1:T(8,128)(2,1)}, ...), branch_computations={%region_1.1_spmd, %region_2.4_spmd} | conditional | flops 433331456 | bytes 30565576 | solution.py:79
  268.4 1.1 fusion.50
  269.5 2.9 fusion.4
  272.4 2.3 fusion.3
  274.8 2.5 fusion.8
  277.3 0.9 copy-done.3
  291.6 1.9 divide_convert_fusion
  294.4 1.4 fusion.51
  295.8 1.4 fusion.42
  297.2 8.7 %all_gather.19 = bf16[192,512]{1,0:T(8,128)(2,1)S(1)} all-gather(bf16[192,128]{1,0:T(8,128)(2,1)S(1)} %fusion.42), channel_id=1, replica_groups=mesh['ep'=8,'tp'=4] {'tp'}, dimensions={1}, use_global_device_ids=true | all-gather | bytes 245760 | tf_op jit(solution)/shard_map/all_gather | solution.py:134
  305.9 2.6 copy.44
  308.5 2.1 reshape.120
  310.7 3.3 gather_fusion.1
  313.9 2.5 reshape.122
  316.4 2.4 multiply_reduce_fusion
  318.9 1.0 fusion.41
  319.8 117.7 %all-gather.7.cloned.1.call-done = bf16[768,1024]{0,1:T(8,128)(2,1)} async-done(((bf16[768,256]{0,1:T(8,128)(2,1)}), bf16[768,1024]{0,1:T(8,128)(2,1)}) %all-gather.7.cloned.1.call-update) | async-done | bytes 1572880 | tf_op jit(solution)/shard_map/all_gather | solution.py:133
  437.5 3.6 convolution_convert_fusion
  (98 shorter events, 14.4 us)
Async XLA Ops:
  7.2 154.2 %copy-start = (bf16[4,512,512]{2,1,0:T(8,128)(2,1)S(1)}, bf16[4,512,512]{2,1,0:T(8,128)(2,1)}, u32[]{:S(2)}) copy-start(bf16[4,512,512]{2,1,0:T(8,128)(2,1)} %param.30) | copy-start | bytes 6291460
  7.2 117.9 %all-gather.9.cloned.1.call-start = ((), (), s32[]{:S(2)}) async-start(), calls=%async_computation.4 | async-start | bytes 6553600 | tf_op jit(solution)/shard_map/all_gather | solution.py:114
  64.8 96.6 %all-gather.11.cloned.1.call-start = ((), (), s32[]{:S(2)}) async-start(), calls=%async_computation.5 | async-start | bytes 1638400 | tf_op jit(solution)/shard_map/all_gather | solution.py:120
  125.0 4.8 %copy-start.1 = (bf16[8,4,36,2048]{3,2,0,1:T(8,128)(2,1)S(1)}, bf16[8,4,36,2048]{3,2,0,1:T(8,128)(2,1)}, u32[]{:S(2)}) copy-start(bf16[8,4,36,2048]{3,2,0,1:T(8,128)(2,1)} %all-gather.9.cloned.1.call-done) | copy-start | bytes 14155780
  125.0 5.3 %copy-start.7 = (bf16[4,2048,128]{2,1,0:T(8,128)(2,1)S(1)}, bf16[4,2048,128]{2,1,0:T(8,128)(2,1)}, u32[]{:S(2)}) copy-start(bf16[4,2048,128]{2,1,0:T(8,128)(2,1)} %param.29) | copy-start | bytes 6291460
  132.6 119.0 %all-gather.5.cloned.1.call-start = ((), (), s32[]{:S(2)}) async-start(), calls=%async_computation.2 | async-start | bytes 7077888 | tf_op jit(solution)/shard_map/all_gather | solution.py:43
  165.5 140.4 %all-to-all-start.1 = ((bf16[8,4,36,512]{3,1,2,0:T(4,128)(2,1)}), bf16[8,4,36,512]{3,1,2,0:T(4,128)(2,1)}, u32[]{:S(2)}, u32[]{:S(2)}) async-start(bf16[8,4,36,512]{3,1,2,0:T(4,128)(2,1)} %copy.43), calls=%async_computation.1 | async-start | bytes 2359296 | tf_op jit(solution)/shard_map/all_to_all | solution.py:124
  170.1 267.4 %all-gather.7.cloned.1.call-start = ((), (), s32[]{:S(2)}) async-start(), calls=%async_computation.3 | async-start | bytes 1966080 | tf_op jit(solution)/shard_map/all_gather | solution.py:133
  252.6 41.0 %copy-start.6 = (f32[192,3]{0,1:T(4,128)S(1)}, f32[192,3]{0,1:T(4,128)}, u32[]{:S(2)}) copy-start(f32[192,3]{0,1:T(4,128)} %param.27) | copy-start | bytes 6916
  259.6 2.4 copy-start.2
  264.5 0.9 copy-start.3
  272.4 2.4 copy-start.2
  277.3 0.9 copy-start.3
  313.9 2.5 copy-start.5
  313.9 5.0 %copy-start.4 = (bf16[512,512]{1,0:T(8,128)(2,1)S(1)}, bf16[512,512]{1,0:T(8,128)(2,1)}, u32[]{:S(2)}) copy-start(bf16[512,512]{1,0:T(8,128)(2,1)} %param.33) | copy-start | bytes 1572868
Sparse Core Ops, SparseCore 0:
  64.9 60.0 all-gather.8
  132.8 28.5 all-gather.10
  163.5 88.0 all-gather.4
  293.7 143.7 all-gather.6
where the time goes:
time: 450 us; the launch traced here: 448 us
  waiting for transfers between devices  280 us (62%)
  local copies, waits for them, and re-layouts  50.3 us (11%)
  blocking collectives  44.2 us (10%)
  matrix products  27.4 us (6%)
  other arithmetic  16.8 us (4%)
  between operations  14 us (3%)
  loops' own time  9.67 us (2%)
  starting transfers between devices  4.94 us (1%)
    all_gather x1, waiting for transfers between devices, local(): lax.all_gather(heads_out, 'tp', axis=1, tiled=True)  118 us
    all_gather x1, waiting for transfers between devices, local(): shard_rows = lax.all_gather(key_value, 'ep', axis=0, tiled=True)  81.3 us
    all_gather x1, waiting for transfers between devices, local(): arrived = lax.all_gather(arrived, 'tp', axis=3, tiled=True)  60.2 us
    all_to_all x1, blocking collectives, local(): lax.all_to_all(outgoing, 'ep', split_axis=0, concat_axis=0, tiled=True)  35.5 us
    all_gather x1, waiting for transfers between devices, local(): hidden = lax.all_gather(hidden, 'tp', axis=3, tiled=True)  21 us
  transfers between devices with their start and end apart: 5, of which 4 were waited for; matrix products, arithmetic and copies ran while one was open for 13% of the time, Pallas kernels for 0%

commit v1 on v0

--- a/solution.py
+++ b/solution.py
@@ -6,6 +6,17 @@
 HEAD = 64
 neg_fill = -1e30
 norm_eps = 1e-06
+
+
+def gather_by_hops(shard, mesh_axis, d):
+    n_dev = lax.axis_size(mesh_axis)
+    right = [(i, (i + 1) % n_dev) for i in range(n_dev)]
+    parts = [shard]
+    for stride in range(1, n_dev):
+        parts = [lax.ppermute(parts[0], mesh_axis, right), *parts]
+    full = jnp.concatenate(parts, axis=d)
+    shift = (lax.axis_index(mesh_axis) + 1) * parts[-1].shape[d]
+    return jnp.roll(full, shift, axis=d)
 
 
 def local(
@@ -40,7 +51,7 @@
         jnp.zeros((local_heads, row_count), jnp.float32),
         jnp.zeros((local_heads, row_count, HEAD), jnp.float32),
     )
-    shard_rows = lax.all_gather(key_value, "ep", axis=0, tiled=True)
+    shard_rows = gather_by_hops(key_value, "ep", 0)
     piece_len = shard_rows.shape[0]
     key_span = 512
 

time: 450 us -> 412 us (0.916)
  waiting for transfers between devices: 280 us -> 104 us
  starting transfers between devices: 4.94 us -> 105 us
  local copies, waits for them, and re-layouts: 50.3 us -> 89.2 us
    all_gather x1, waiting for transfers between devices: 118 us -> 10.9 us  [local(): lax.all_gather(heads_out, 'tp', axis=1, tiled=True)]
    all_to_all x1, starting transfers between devices: 4.6 us -> 105 us  [local(): lax.all_to_all(result, 'ep', split_axis=0, concat_axis=0, tiled=True)]
    ppermute x0 -> x7, waiting for transfers between devices: none -> 90.1 us  [gather_by_hops(): parts = [lax.ppermute(parts[0], mesh_axis, right), *parts]]
    all_gather x1 -> x0, waiting for transfers between devices: 81.3 us -> none  [local(): shard_rows = lax.all_gather(key_value, 'ep', axis=0, tiled=True)]
    all_gather x1, waiting for transfers between devices: 60.2 us -> 0.01 us  [local(): arrived = lax.all_gather(arrived, 'tp', axis=3, tiled=True)]
    unnamed x17 -> x51, local copies, waits for them, and re-layouts: 7.06 us -> 37.1 us
    all_gather x1, waiting for transfers between devices: 21 us -> 0.02 us  [local(): hidden = lax.all_gather(hidden, 'tp', axis=3, tiled=True)]
    dynamic_slice x0 -> x1, local copies, waits for them, and re-layouts: none -> 9.54 us  [gather_by_hops(): return jnp.roll(full, shift, axis=d)]
  transfers between devices with their start and end apart: 5 -> 11, of which waited for: 4 -> 9; matrix products, arithmetic and copies ran while one was open for 13% -> 20% of each run, Pallas kernels for 0% -> 0%
where the time goes in v1:
time: 412 us; the launch traced here: 410 us
  starting transfers between devices  105 us (25%)
  waiting for transfers between devices  104 us (25%)
  local copies, waits for them, and re-layouts  89.2 us (22%)
  blocking collectives  44.3 us (11%)
  matrix products  26.6 us (6%)
  other arithmetic  17.8 us (4%)
  between operations  14 us (3%)
  loops' own time  8.71 us (2%)
    all_to_all x1, starting transfers between devices, local(): lax.all_to_all(result, 'ep', split_axis=0, concat_axis=0, tiled=True)  105 us
    ppermute x7, waiting for transfers between devices, gather_by_hops(): parts = [lax.ppermute(parts[0], mesh_axis, right), *parts]  90.1 us
    unnamed x51, local copies, waits for them, and re-layouts  37.1 us
    all_to_all x1, blocking collectives, local(): lax.all_to_all(outgoing, 'ep', split_axis=0, concat_axis=0, tiled=True)  35.5 us
    all_gather x1, waiting for transfers between devices, local(): lax.all_gather(heads_out, 'tp', axis=1, tiled=True)  10.9 us
    dynamic_slice x1, local copies, waits for them, and re-layouts, gather_by_hops(): return jnp.roll(full, shift, axis=d)  9.54 us
    all_gather x1, blocking collectives, local(): lax.all_gather(shared_hidden, 'tp', axis=1, tiled=True)  8.74 us
  transfers between devices with their start and end apart: 11, of which 9 were waited for; matrix products, arithmetic and copies ran while one was open for 20% of the time, Pallas kernels for 0%

profile of v1, /device:TPU:0, one launch (start us, length us, event | category | flops | bytes accessed | tf_op | source)
XLA Modules:
  0.0 409.6 jit_solution(5757200894351019977)
XLA Ops:
  12.8 4.1 %scatter_custom_fusion = s32[1152]{0:T(1024)S(1)} fusion(s32[576]{0:T(1024)S(1)} %fusion.49, s32[576]{0:T(1024)S(1)} %add_select_fusion, s32[]{:T(128)} %constant.98.clone.1), kind=kCustom, calls=%fused_computation.83 | custom fusion | bytes 4612 | tf_op jit(solution)/shard_map/scatter | solution.py:119
  18.3 4.7 %gather_fusion = bf16[1152,512]{1,0:T(8,128)(2,1)} fusion(bf16[193,512]{1,0:T(8,128)(2,1)S(1)} %pad_dynamic-slice_fusion, s32[2048]{0:T(1024)S(1)} %pad_clamp_fusion), kind=kCustom, calls=%fused_computation | custom fusion | bytes 2363904 | tf_op jit(solution)/shard_map/gather | solution.py:122
  23.0 3.0 reshape.119
  25.9 1.9 copy.41
  27.9 35.5 %all_to_all.10 = bf16[8,4,36,512]{3,1,2,0:T(4,128)(2,1)S(1)} all-to-all(bf16[8,4,36,512]{3,1,2,0:T(4,128)(2,1)S(1)} %copy.41), channel_id=1, replica_groups=mesh['ep'=8,'tp'=4] {'ep'}, dimensions={0} | all-to-all | bytes 2359296 | tf_op jit(solution)/shard_map/all_to_all | solution.py:124
  69.0 13.2 %collective-permute-done = bf16[768,512]{0,1:T(8,128)(2,1)S(1)} collective-permute-done((bf16[768,512]{0,1:T(8,128)(2,1)S(1)}, bf16[768,512]{0,1:T(8,128)(2,1)S(1)}, u32[]{:S(2)}, u32[]{:S(2)}) %collective-permute-start) | collective-permute-done | bytes 786464 | tf_op jit(solution)/shard_map/ppermute | solution.py:16
  83.1 13.2 %collective-permute-done.1 = bf16[768,512]{0,1:T(8,128)(2,1)S(1)} collective-permute-done((bf16[768,512]{0,1:T(8,128)(2,1)S(1)}, bf16[768,512]{0,1:T(8,128)(2,1)S(1)}, u32[]{:S(2)}, u32[]{:S(2)}) %collective-permute-start.1) | collective-permute-done | bytes 786464 | tf_op jit(solution)/shard_map/ppermute | solution.py:16
  97.2 13.2 %collective-permute-done.2 = bf16[768,512]{0,1:T(8,128)(2,1)S(1)} collective-permute-done((bf16[768,512]{0,1:T(8,128)(2,1)S(1)}, bf16[768,512]{0,1:T(8,128)(2,1)S(1)}, u32[]{:S(2)}, u32[]{:S(2)}) %collective-permute-start.2) | collective-permute-done | bytes 786464 | tf_op jit(solution)/shard_map/ppermute | solution.py:16
  111.3 13.2 %collective-permute-done.3 = bf16[768,512]{0,1:T(8,128)(2,1)S(1)} collective-permute-done((bf16[768,512]{0,1:T(8,128)(2,1)S(1)}, bf16[768,512]{0,1:T(8,128)(2,1)S(1)}, u32[]{:S(2)}, u32[]{:S(2)}) %collective-permute-start.3) | collective-permute-done | bytes 786464 | tf_op jit(solution)/shard_map/ppermute | solution.py:16
  125.5 13.2 %collective-permute-done.4 = bf16[768,512]{0,1:T(8,128)(2,1)S(1)} collective-permute-done((bf16[768,512]{0,1:T(8,128)(2,1)S(1)}, bf16[768,512]{0,1:T(8,128)(2,1)S(1)}, u32[]{:S(2)}, u32[]{:S(2)}) %collective-permute-start.4) | collective-permute-done | bytes 786464 | tf_op jit(solution)/shard_map/ppermute | solution.py:16
  139.5 13.3 %collective-permute-done.5 = bf16[768,512]{0,1:T(8,128)(2,1)} collective-permute-done((bf16[768,512]{0,1:T(8,128)(2,1)S(1)}, bf16[768,512]{0,1:T(8,128)(2,1)}, u32[]{:S(2)}, u32[]{:S(2)}) %collective-permute-start.5) | collective-permute-done | bytes 786464 | tf_op jit(solution)/shard_map/ppermute | solution.py:16
  152.9 1.9 copy.36
  155.7 10.7 %collective-permute-done.6 = bf16[768,512]{0,1:T(8,128)(2,1)} collective-permute-done((bf16[768,512]{0,1:T(8,128)(2,1)}, bf16[768,512]{0,1:T(8,128)(2,1)}, u32[]{:S(2)}, u32[]{:S(2)}) %collective-permute-start.6) | collective-permute-done | bytes 786464 | tf_op jit(solution)/shard_map/ppermute | solution.py:16
  166.4 2.1 constant_dynamic-update-slice_fusion.15
  168.5 2.1 constant_dynamic-update-slice_fusion.14
  170.6 2.1 constant_dynamic-update-slice_fusion.13
  172.7 2.1 constant_dynamic-update-slice_fusion.12
  178.8 2.1 constant_dynamic-update-slice_fusion.7
  180.9 2.2 constant_dynamic-update-slice_fusion.6
  183.2 4.8 %fusion.29 = f32[8,4,36,128]{3,2,0,1:T(8,128)S(1)} fusion(bf16[8,4,36,2048]{3,2,0,1:T(8,128)(2,1)} %all-gather.6.cloned.1.call-done, bf16[4,2048,128]{2,1,0:T(8,128)(2,1)} %param.28), kind=kOutput, calls=%fused_computation.37 | convolution fusion | flops 603979776 | bytes 7405568 | tf_op jit(solution)/shard_map/aecd,edf->aecf/dot_general | solution.py:126
  188.5 2.3 fusion.38
  191.1 2.2 constant_dynamic-update-slice_fusion.5
  193.3 2.2 constant_dynamic-update-slice_fusion.4
  195.4 2.1 constant_dynamic-update-slice_fusion.3
  197.6 2.1 constant_dynamic-update-slice_fusion.2
  201.7 9.5 %constant_dynamic-slice_fusion.3 = bf16[6144,512]{0,1:T(8,128)(2,1)} fusion(bf16[12288,512]{0,1:T(8,128)(2,1)} %constant_dynamic-update-slice_fusion, s32[]{:T(128)S(6)} %select_n.52), kind=kLoop, calls=%fused_computation.91 | loop fusion | bytes 12582916 | tf_op jit(solution)/shard_map/jit(_roll_dynamic)/dynamic_slice | solution.py:19
  212.2 35.4 %while.15 = (s32[]{:T(128)}, f32[4,768]{1,0:T(4,128)S(1)}, f32[4,768]{1,0:T(4,128)S(1)}, f32[4,768,64]{1,2,0:T(8,128)}, s32[12]{0:T(128)S(1)}, /*index=5*/s32[]{...) while((s32[]{:T(128)}, f32[4,768]{1,0:T(4,128)S(1)}, ...), condition=%wide.region_5.6_spmd.clone, body=%wide.region_0.5_spmd.clone.sunk | while | flops 433331456 | bytes 30568924 | solution.py:93
  213.3 10.5 %conditional.3 = ((f32[4,768]{1,0:T(4,128)S(1)}, f32[4,768]{1,0:T(4,128)S(1)}, f32[4,768,64]{1,2,0:T(8,128)})) conditional(s32[]{:T(128)} %convert_element_type.85, (f32[4,768]{1,0:T(4,128)S(1)}, f32[4,768]{1,0:T(4,128)S(1)}, f32[4,768,64]{1,2,0:T(8,128)}) %tuple.39, (s32[]{:T(128)}, s32[]{:T(128)}, s32[]{:T(128)}, bf16[6144,512]{0,1:T(8,128)(2,1)}, ...), branch_computations={%region_1.1_spmd, %region_2.4_spmd} | conditional | flops 433331456 | bytes 30565576 | solution.py:90
  216.1 1.9 fusion.4
  218.1 2.3 fusion.3
  220.4 2.5 fusion.8
  225.0 10.5 %conditional.3 = ((f32[4,768]{1,0:T(4,128)S(1)}, f32[4,768]{1,0:T(4,128)S(1)}, f32[4,768,64]{1,2,0:T(8,128)})) conditional(s32[]{:T(128)} %convert_element_type.85, (f32[4,768]{1,0:T(4,128)S(1)}, f32[4,768]{1,0:T(4,128)S(1)}, f32[4,768,64]{1,2,0:T(8,128)}) %tuple.39, (s32[]{:T(128)}, s32[]{:T(128)}, s32[]{:T(128)}, bf16[6144,512]{0,1:T(8,128)(2,1)}, ...), branch_computations={%region_1.1_spmd, %region_2.4_spmd} | conditional | flops 433331456 | bytes 30565576 | solution.py:90
  229.7 2.3 fusion.3
  232.1 2.5 fusion.8
  247.6 1.9 divide_convert_fusion
  249.6 2.2 fusion.26
  251.8 1.9 copy.43
  253.7 104.9 %all-to-all-start.1 = ((bf16[8,4,36,512]{3,1,2,0:T(4,128)(2,1)}), bf16[8,4,36,512]{3,1,2,0:T(4,128)(2,1)}, u32[]{:S(2)}, u32[]{:S(2)}) async-start(bf16[8,4,36,512]{3,1,2,0:T(4,128)(2,1)} %copy.43), calls=%async_computation.1 | async-start | bytes 2359296 | tf_op jit(solution)/shard_map/all_to_all | solution.py:135
  362.2 8.7 %all_gather.15 = bf16[192,512]{1,0:T(8,128)(2,1)S(1)} all-gather(bf16[192,128]{1,0:T(8,128)(2,1)S(1)} %fusion.42), channel_id=1, replica_groups=mesh['ep'=8,'tp'=4] {'tp'}, dimensions={1}, use_global_device_ids=true | all-gather | bytes 245760 | tf_op jit(solution)/shard_map/all_gather | solution.py:145
  371.0 10.9 %all-gather.4.cloned.1.call-done = bf16[768,1024]{0,1:T(8,128)(2,1)} async-done(((bf16[768,256]{0,1:T(8,128)(2,1)}), bf16[768,1024]{0,1:T(8,128)(2,1)}) %all-gather.4.cloned.1.call-update) | async-done | bytes 1572880 | tf_op jit(solution)/shard_map/all_gather | solution.py:144
  381.9 3.6 convolution_convert_fusion
  385.5 2.6 all-to-all-done.1
  388.1 2.6 copy.44
  390.7 2.1 reshape.120
  392.9 3.3 gather_fusion.1
  396.1 2.5 reshape.122
  398.6 2.4 multiply_reduce_fusion
  401.1 2.0 fusion.41
  (146 shorter events, 44.3 us)
Async XLA Ops:
  7.2 242.4 %copy-start = (bf16[4,512,512]{2,1,0:T(8,128)(2,1)S(1)}, bf16[4,512,512]{2,1,0:T(8,128)(2,1)}, u32[]{:S(2)}) copy-start(bf16[4,512,512]{2,1,0:T(8,128)(2,1)} %param.30) | copy-start | bytes 6291460
  7.2 176.0 %all-gather.6.cloned.1.call-start = ((), (), s32[]{:S(2)}) async-start(), calls=%async_computation.3 | async-start | bytes 6553600 | tf_op jit(solution)/shard_map/all_gather | solution.py:125
  64.8 184.8 %all-gather.8.cloned.1.call-start = ((), (), s32[]{:S(2)}) async-start(), calls=%async_computation.4 | async-start | bytes 1638400 | tf_op jit(solution)/shard_map/all_gather | solution.py:131
  68.9 13.3 %collective-permute-start = (bf16[768,512]{0,1:T(8,128)(2,1)S(1)}, bf16[768,512]{0,1:T(8,128)(2,1)S(1)}, u32[]{:S(2)}, u32[]{:S(2)}) collective-permute-start(bf16[768,512]{0,1:T(8,128)(2,1)S(1)} %pad_maximum_fusion), channel_id=1, source_target_pairs={{0,4},{4,8},{8,12},{12,16},{16,20},{20,24},{24,28},{28,0},{1,5},{5... | collective-permute-start | bytes 2359304 | tf_op jit(solution)/shard_map/ppermute | solution.py:16
  82.2 0.9 copy-start.4
  83.1 13.2 %collective-permute-start.1 = (bf16[768,512]{0,1:T(8,128)(2,1)S(1)}, bf16[768,512]{0,1:T(8,128)(2,1)S(1)}, u32[]{:S(2)}, u32[]{:S(2)}) collective-permute-start(bf16[768,512]{0,1:T(8,128)(2,1)S(1)} %collective-permute-done), channel_id=1, source_target_pairs={{0,4},{4,8},{8,12},{12,16},{16,20},{20,24},{24,28},{28,0},{1,5},{5... | collective-permute-start | bytes 2359304 | tf_op jit(solution)/shard_map/ppermute | solution.py:16
  96.3 0.9 copy-start.7
  97.2 13.2 %collective-permute-start.2 = (bf16[768,512]{0,1:T(8,128)(2,1)S(1)}, bf16[768,512]{0,1:T(8,128)(2,1)S(1)}, u32[]{:S(2)}, u32[]{:S(2)}) collective-permute-start(bf16[768,512]{0,1:T(8,128)(2,1)S(1)} %collective-permute-done.1), channel_id=1, source_target_pairs={{0,4},{4,8},{8,12},{12,16},{16,20},{20,24},{24,28},{28,0},{1,5},{5... | collective-permute-start | bytes 2359304 | tf_op jit(solution)/shard_map/ppermute | solution.py:16
  110.4 0.9 copy-start.9
  111.3 13.2 %collective-permute-start.3 = (bf16[768,512]{0,1:T(8,128)(2,1)S(1)}, bf16[768,512]{0,1:T(8,128)(2,1)S(1)}, u32[]{:S(2)}, u32[]{:S(2)}) collective-permute-start(bf16[768,512]{0,1:T(8,128)(2,1)S(1)} %collective-permute-done.2), channel_id=1, source_target_pairs={{0,4},{4,8},{8,12},{12,16},{16,20},{20,24},{24,28},{28,0},{1,5},{5... | collective-permute-start | bytes 2359304 | tf_op jit(solution)/shard_map/ppermute | solution.py:16
  124.5 0.9 copy-start.11
  125.5 13.2 %collective-permute-start.4 = (bf16[768,512]{0,1:T(8,128)(2,1)S(1)}, bf16[768,512]{0,1:T(8,128)(2,1)S(1)}, u32[]{:S(2)}, u32[]{:S(2)}) collective-permute-start(bf16[768,512]{0,1:T(8,128)(2,1)S(1)} %collective-permute-done.3), channel_id=1, source_target_pairs={{0,4},{4,8},{8,12},{12,16},{16,20},{20,24},{24,28},{28,0},{1,5},{5... | collective-permute-start | bytes 2359304 | tf_op jit(solution)/shard_map/ppermute | solution.py:16
  138.7 0.9 copy-start.12
  139.5 13.3 %collective-permute-start.5 = (bf16[768,512]{0,1:T(8,128)(2,1)S(1)}, bf16[768,512]{0,1:T(8,128)(2,1)}, u32[]{:S(2)}, u32[]{:S(2)}) collective-permute-start(bf16[768,512]{0,1:T(8,128)(2,1)S(1)} %collective-permute-done.4), channel_id=1, source_target_pairs={{0,4},{4,8},{8,12},{12,16},{16,20},{20,24},{24,28},{28,0},{1,5},{5... | collective-permute-start | bytes 2359304 | tf_op jit(solution)/shard_map/ppermute | solution.py:16
  152.9 13.5 %collective-permute-start.6 = (bf16[768,512]{0,1:T(8,128)(2,1)}, bf16[768,512]{0,1:T(8,128)(2,1)}, u32[]{:S(2)}, u32[]{:S(2)}) collective-permute-start(bf16[768,512]{0,1:T(8,128)(2,1)} %collective-permute-done.5), channel_id=1, source_target_pairs={{0,4},{4,8},{8,12},{12,16},{16,20},{20,24},{24,28},{28,0},{1,5},{5... | collective-permute-start | bytes 2359304 | tf_op jit(solution)/shard_map/ppermute | solution.py:16
  154.8 20.0 %copy-start.10 = (bf16[768,512]{0,1:T(8,128)(2,1)S(1)}, bf16[768,512]{0,1:T(8,128)(2,1)}, u32[]{:S(2)}) copy-start(bf16[768,512]{0,1:T(8,128)(2,1)} %copy-done.9) | copy-start | bytes 2359300
  154.8 21.0 %copy-start.8 = (bf16[768,512]{0,1:T(8,128)(2,1)S(1)}, bf16[768,512]{0,1:T(8,128)(2,1)}, u32[]{:S(2)}) copy-start(bf16[768,512]{0,1:T(8,128)(2,1)} %copy-done.7) | copy-start | bytes 2359300
  154.8 22.0 %copy-start.5 = (bf16[768,512]{0,1:T(8,128)(2,1)S(1)}, bf16[768,512]{0,1:T(8,128)(2,1)}, u32[]{:S(2)}) copy-start(bf16[768,512]{0,1:T(8,128)(2,1)} %copy-done.4) | copy-start | bytes 2359300
  154.8 23.0 %copy-start.1 = (bf16[768,256]{0,1:T(8,128)(2,1)S(1)}, bf16[768,256]{0,1:T(8,128)(2,1)}, u32[]{:S(2)}) copy-start(bf16[768,256]{0,1:T(8,128)(2,1)} %copy.35) | copy-start | bytes 1179652
  183.2 4.8 %copy-start.3 = (bf16[8,4,36,2048]{3,2,0,1:T(8,128)(2,1)S(1)}, bf16[8,4,36,2048]{3,2,0,1:T(8,128)(2,1)}, u32[]{:S(2)}) copy-start(bf16[8,4,36,2048]{3,2,0,1:T(8,128)(2,1)} %all-gather.6.cloned.1.call-done) | copy-start | bytes 14155780
  183.2 5.3 %copy-start.17 = (bf16[4,2048,128]{2,1,0:T(8,128)(2,1)S(1)}, bf16[4,2048,128]{2,1,0:T(8,128)(2,1)}, u32[]{:S(2)}) copy-start(bf16[4,2048,128]{2,1,0:T(8,128)(2,1)} %param.29) | copy-start | bytes 6291460
  190.8 191.1 %all-gather.4.cloned.1.call-start = ((), (), s32[]{:S(2)}) async-start(), calls=%async_computation.2 | async-start | bytes 1966080 | tf_op jit(solution)/shard_map/all_gather | solution.py:144
  191.0 8.7 %copy-start.6 = (bf16[768,512]{0,1:T(8,128)(2,1)S(1)}, bf16[768,512]{0,1:T(8,128)(2,1)}, u32[]{:S(2)}) copy-start(bf16[768,512]{0,1:T(8,128)(2,1)} %copy-done.4) | copy-start | bytes 2359300
  191.0 9.6 %copy-start.2 = (bf16[768,256]{0,1:T(8,128)(2,1)S(1)}, bf16[768,256]{0,1:T(8,128)(2,1)}, u32[]{:S(2)}) copy-start(bf16[768,256]{0,1:T(8,128)(2,1)} %copy.35) | copy-start | bytes 1179652
  201.7 10.5 %copy-start.15 = (bf16[768,256]{0,1:T(8,128)(2,1)S(1)}, bf16[768,256]{0,1:T(8,128)(2,1)}, u32[]{:S(2)}) copy-start(bf16[768,256]{0,1:T(8,128)(2,1)} %copy.36) | copy-start | bytes 1179652
  216.1 4.3 %copy-start.13 = (f32[4,768,64]{1,2,0:T(8,128)S(1)}, f32[4,768,64]{1,2,0:T(8,128)}, u32[]{:S(2)}) copy-start(f32[4,768,64]{1,2,0:T(8,128)} %get-tuple-element.79) | copy-start | bytes 2359300 | tf_op jit(solution)/shard_map/while/body/eval_jaxpr/cond
  222.9 0.9 copy-start.14
  227.8 4.3 %copy-start.13 = (f32[4,768,64]{1,2,0:T(8,128)S(1)}, f32[4,768,64]{1,2,0:T(8,128)}, u32[]{:S(2)}) copy-start(f32[4,768,64]{1,2,0:T(8,128)} %get-tuple-element.79) | copy-start | bytes 2359300 | tf_op jit(solution)/shard_map/while/body/eval_jaxpr/cond
  234.6 0.9 copy-start.14
  247.6 111.1 %copy-start.16 = (f32[192,3]{0,1:T(4,128)S(1)}, f32[192,3]{0,1:T(4,128)}, u32[]{:S(2)}) copy-start(f32[192,3]{0,1:T(4,128)} %param.27) | copy-start | bytes 6916
  253.7 134.4 %all-to-all-start.1 = ((bf16[8,4,36,512]{3,1,2,0:T(4,128)(2,1)}), bf16[8,4,36,512]{3,1,2,0:T(4,128)(2,1)}, u32[]{:S(2)}, u32[]{:S(2)}) async-start(bf16[8,4,36,512]{3,1,2,0:T(4,128)(2,1)} %copy.43), calls=%async_computation.1 | async-start | bytes 2359296 | tf_op jit(solution)/shard_map/all_to_all | solution.py:135
Sparse Core Ops, SparseCore 0:
  64.9 60.0 all-gather.5
  190.9 26.7 all-gather.7
  249.7 132.1 all-gather.3
